TPU v7x, 32 devices: a whole 2x2x4 slice. The times are simulated.
32 devices in a mesh: fs: 8 (over z, x), tp: 4 (over y, core).
Axes of the slice: x: 2, y: 2, z: 4, core: 2. Of those that a mesh axis runs over, the one named last changes fastest.
Arguments:
- tokens: bfloat16 [8192, 2048], P('fs', 'tp'), may hold values from -6 to 6
- recurrence_norm_gain: float32 [2048], replicated, may hold values from 0.1 to 1.9
- output_gate_weight: bfloat16 [2048, 2816], P('fs', 'tp'), may hold values from -0.125 to 0.125
- recurrence_input_weight: bfloat16 [2048, 2816], P('fs', 'tp'), may hold values from -0.125 to 0.125
- convolution_taps: float32 [4, 2816], P(None, 'tp'), may hold values from -3 to 3
- recurrence_gate_weight: bfloat16 [8, 352, 352], P('tp'), may hold values from -0.3125 to 0.3125
- input_gate_weight: bfloat16 [8, 352, 352], P('tp'), may hold values from -0.3125 to 0.3125
- base_decay_logit: float32 [2816], P('tp'), may hold values from 4.5 to 9.5
- token_log_decay: float32 [8192], P('fs'), may hold values from -0.7 to 0, as said below
- recurrence_output_weight: bfloat16 [2816, 2048], P('tp', 'fs'), may hold values from -0.4375 to 0.4375
- feedforward_norm_gain: float32 [2048], replicated, may hold values from 0.1 to 1.9
- feedforward_gate_weight: bfloat16 [2048, 5632], P('fs', 'tp'), may hold values from -0.125 to 0.125
- feedforward_up_weight: bfloat16 [2048, 5632], P('fs', 'tp'), may hold values from -0.125 to 0.125
- feedforward_down_weight: bfloat16 [5632, 2048], P('tp', 'fs'), may hold values from -0.15625 to 0.15625
Outputs:
- layer_out: bfloat16 [8192, 2048], P('fs', 'tp')
Inputs may be any that keep to these rules, and one draw needn't show every extreme that they name: `token_log_decay`: each entry is zero or lies between -0.7 and -0.22.
All inputs are finite; a program needn't handle non-finite values.
Results may differ from a plain program's by a relative error of at most 0.022.
Values may be sent and summed in bfloat16 or wider, within the bound.
No kernel may reach another device: no remote copies, remote signals or barrier semaphores. Data moves between devices by JAX's collectives and lax.ppermute only.
A program may use at most 128 MiB of HBM per device.

v0:
```python
import jax
import jax.numpy as jnp
from jax import lax
from jax.sharding import PartitionSpec as P

LEN = 128


EPSILON = 1e-06
GATE_EXPONENT = 8.0


def norm_rows(values, gain_vec):
    widened = values.astype(jnp.float32)
    scaled = widened * lax.rsqrt(jnp.mean(widened * widened, axis=-1, keepdims=True) + EPSILON)
    return (scaled * gain_vec).astype(jnp.bfloat16)


def causal_taps(feature_vector, convolution_taps, length):
    row_count, channels = feature_vector.shape
    tap_count = convolution_taps.shape[0]
    blocks = feature_vector.reshape(row_count // length, length, channels)
    target = lax.broadcasted_iota(jnp.int32, (tap_count, length, length), 1)
    source = lax.broadcasted_iota(jnp.int32, (tap_count, length, length), 2)
    offset = lax.broadcasted_iota(jnp.int32, (tap_count, length, length), 0)
    shifters = (source == target - (tap_count - 1) + offset).astype(jnp.bfloat16)
    shifted = jnp.einsum("kts,bsc->kbtc", shifters, blocks, preferred_element_type=jnp.float32)
    summed = convolution_taps[0] * shifted[0]
    for position in range(1, tap_count):
        summed = summed + convolution_taps[position] * shifted[position]
    return summed.reshape(row_count, channels).astype(jnp.bfloat16)


def combine_steps(earlier, latter):
    return (earlier[0] * latter[0], latter[0] * earlier[1] + latter[1])


def linear_scan(decays, driven, length):
    row_count, channels = decays.shape
    shaped = (
        decays.reshape(row_count // length, length, channels),
        driven.reshape(row_count // length, length, channels),
    )
    result = lax.associative_scan(combine_steps, shaped, axis=1)
    return result[1].reshape(row_count, channels)


def block_dense(weight):
    groups, block_width, _ = weight.shape
    identity = jnp.eye(groups, dtype=jnp.bfloat16)[:, None, :, None]
    return (weight[:, :, None, :] * identity).reshape(groups * block_width, groups * block_width)


def two_projections(normed, collected):
    return (
        jnp.dot(normed, collected[0], preferred_element_type=jnp.float32),
        jnp.dot(normed, collected[1], preferred_element_type=jnp.float32),
    )


def project_down(values, weight):
    return jnp.dot(
        values, lax.all_gather(weight, "fs", axis=1, tiled=True), preferred_element_type=jnp.float32
    )


def recurrence(
    gate_projected,
    feature_vector,
    convolution_taps,
    recurrence_gate_weight,
    input_gate_weight,
    base_decay_logit,
    token_log_decay,
):
    mixed_in = causal_taps(feature_vector, convolution_taps, LEN)
    recurrence_gate = jax.nn.sigmoid(
        jnp.dot(mixed_in, block_dense(recurrence_gate_weight), preferred_element_type=jnp.float32)
    )
    inject_gate = jax.nn.sigmoid(
        jnp.dot(mixed_in, block_dense(input_gate_weight), preferred_element_type=jnp.float32)
    )
    decay_log_value = (
        -GATE_EXPONENT * jax.nn.softplus(-base_decay_logit)[None, :] * recurrence_gate
        + token_log_decay[:, None]
    )
    decays = jnp.exp(decay_log_value)
    driven = jnp.sqrt(-jnp.expm1(2.0 * decay_log_value)) * (
        inject_gate * mixed_in.astype(jnp.float32)
    )
    states = linear_scan(decays, driven, LEN)
    return (states * jax.nn.gelu(gate_projected)).astype(jnp.bfloat16)


def shards(
    tokens,
    recurrence_norm_gain,
    output_gate_weight,
    recurrence_input_weight,
    convolution_taps,
    recurrence_gate_weight,
    input_gate_weight,
    base_decay_logit,
    token_log_decay,
    recurrence_output_weight,
    feedforward_norm_gain,
    feedforward_gate_weight,
    feedforward_up_weight,
    feedforward_down_weight,
):
    collected = (
        lax.all_gather(output_gate_weight, "fs", axis=0, tiled=True),
        lax.all_gather(recurrence_input_weight, "fs", axis=0, tiled=True),
        lax.all_gather(feedforward_gate_weight, "fs", axis=0, tiled=True),
        lax.all_gather(feedforward_up_weight, "fs", axis=0, tiled=True),
    )
    full_rows = lax.all_gather(tokens, "tp", axis=1, tiled=True)
    normed = norm_rows(full_rows, recurrence_norm_gain)
    gate_projected, feature_vector = two_projections(normed, collected[0:2])
    carried = recurrence(
        gate_projected,
        feature_vector.astype(jnp.bfloat16),
        convolution_taps,
        recurrence_gate_weight,
        input_gate_weight,
        base_decay_logit,
        token_log_decay,
    )
    mixer_term = project_down(carried, recurrence_output_weight)
    own_sum = lax.psum_scatter(
        mixer_term.astype(jnp.bfloat16), "tp", scatter_dimension=1, tiled=True
    ).astype(jnp.float32)
    residual_own = (tokens.astype(jnp.float32) + own_sum).astype(jnp.bfloat16)
    residual_full = lax.all_gather(residual_own, "tp", axis=1, tiled=True)
    normed_two = norm_rows(residual_full, feedforward_norm_gain)
    gate_hidden, up_hidden = two_projections(normed_two, collected[2:4])
    hidden = (jax.nn.silu(gate_hidden) * up_hidden).astype(jnp.bfloat16)
    down_term = project_down(hidden, feedforward_down_weight)
    own_down = lax.psum_scatter(
        down_term.astype(jnp.bfloat16), "tp", scatter_dimension=1, tiled=True
    ).astype(jnp.float32)
    return (residual_own.astype(jnp.float32) + own_down).astype(jnp.bfloat16)


def solution(mesh):
    in_specs = (
        P("fs", "tp"),
        P(),
        P("fs", "tp"),
        P("fs", "tp"),
        P(None, "tp"),
        P("tp", None, None),
        P("tp", None, None),
        P("tp"),
        P("fs"),
        P("tp", "fs"),
        P(),
        P("fs", "tp"),
        P("fs", "tp"),
        P("tp", "fs"),
    )
    out_specs = P("fs", "tp")
    return jax.shard_map(shards, mesh=mesh, in_specs=in_specs, out_specs=out_specs, check_vma=False)
```

profile of v0, /device:TPU:0, one launch (start us, length us, event | category | flops | bytes accessed | tf_op | source)
XLA Modules:
  0.0 1082.4 jit_solution(1734964078290439983)
XLA Ops:
  10.3 3.4 broadcast_multiply_fusion
  15.5 30.6 %all-gather.9.cloned.1.call-done = bf16[1024,2048]{1,0:T(8,128)(2,1)} async-done(((bf16[1024,512]{1,0:T(8,128)(2,1)}), bf16[1024,2048]{1,0:T(8,128)(2,1)}) %all-gather.9.cloned.1.call-update) | async-done | bytes 4194320 | tf_op jit(solution)/shard_map/all_gather | solution.py:117
  46.1 3.1 fusion
  49.2 58.5 %all-gather.11.cloned.1.call-done = bf16[2048,704]{0,1:T(8,128)(2,1)} async-done(((bf16[256,704]{0,1:T(8,128)(2,1)}), bf16[2048,704]{0,1:T(8,128)(2,1)}) %all-gather.11.cloned.1.call-update) | async-done | bytes 2883600 | tf_op jit(solution)/shard_map/all_gather | solution.py:113
  107.7 6.3 fusion.20
  114.5 1.8 convolution_bitcast_fusion
  116.3 2.9 fusion.57
  119.2 0.9 copy.46
  120.1 1.7 copy.47
  121.8 1.7 copy.48
  123.5 1.7 copy.49
  125.2 1.7 copy.50
  126.9 1.8 multiply_add_fusion
  128.6 5.0 multiply_bitcast_fusion
  134.3 51.8 %slice.194 = f32[8,64,704]{1,0,2:T(8,128)} slice(f32[8,128,704]{1,0,2:T(8,128)S(1)} %bitcast.97), slice={[0:8:1], [0:127:2], [0:704:1]} | slice | bytes 2883584 | tf_op jit(solution)/shard_map/slice | solution.py:44
  186.1 56.3 %slice.195 = f32[8,64,704]{1,0,2:T(8,128)} slice(f32[8,128,704]{1,0,2:T(8,128)S(1)} %bitcast.98), slice={[0:8:1], [1:128:2], [0:704:1]} | slice | bytes 2883584 | tf_op jit(solution)/shard_map/slice | solution.py:44
  242.4 2.2 exponential_bitcast_fusion
  244.6 2.4 copy.76
  246.9 52.7 %slice.193 = f32[8,64,704]{1,0,2:T(8,128)} slice(f32[8,128,704]{1,0,2:T(8,128)} %bitcast.101), slice={[0:8:1], [1:128:2], [0:704:1]} | slice | bytes 2883584 | tf_op jit(solution)/shard_map/slice | solution.py:44
  299.6 51.8 %slice.197 = f32[8,64,704]{1,0,2:T(8,128)} slice(f32[8,128,704]{1,0,2:T(8,128)} %bitcast.102), slice={[0:8:1], [0:127:2], [0:704:1]} | slice | bytes 2883584 | tf_op jit(solution)/shard_map/slice | solution.py:44
  351.5 55.5 %slice.241 = f32[8,63,704]{1,0,2:T(8,128)} slice(f32[8,128,704]{1,0,2:T(8,128)S(1)} %bitcast.99), slice={[0:8:1], [2:128:2], [0:704:1]} | slice | bytes 2838528 | tf_op jit(solution)/shard_map/slice | solution.py:44
  407.0 52.1 %slice.192 = f32[8,63,704]{1,0,2:T(8,128)} slice(f32[8,128,704]{1,0,2:T(8,128)} %bitcast.103), slice={[0:8:1], [2:128:2], [0:704:1]} | slice | bytes 2838528 | tf_op jit(solution)/shard_map/slice | solution.py:44
  459.1 3.3 copy.65
  462.3 3.3 copy.66
  465.6 3.3 copy.64
  468.9 3.3 copy.67
  472.1 3.2 fusion.58
  480.7 1.5 pad.48
  482.2 1.0 fusion.47
  483.2 1.4 pad_maximum_fusion.4
  484.6 3.4 pad.47
  488.0 1.6 add.195
  489.6 1.0 fusion.45
  490.8 5.0 pad.50
  495.7 1.8 add.197
  497.5 8.9 pad.52
  506.5 1.3 fusion.42
  507.8 5.8 pad.51
  513.5 2.4 add.199
  515.9 2.0 fusion.41
  518.8 16.1 %pad.53 = f32[8,64,704]{2,0,1:T(8,128)} pad(f32[8,32,704]{2,0,1:T(8,128)} %pad_maximum_fusion.1, f32[]{:T(128)} %constant.10.clone.1), padding=0_0_0x0_1_1x0_0_0 | pad | bytes 2162692 | tf_op jit(solution)/shard_map/pad | solution.py:44
  535.0 16.1 %pad.54 = f32[8,64,704]{2,0,1:T(8,128)} pad(f32[8,32,704]{2,0,1:T(8,128)} %add.199, f32[]{:T(128)} %constant.10.clone.1), padding=0_0_0x1_0_1x0_0_0 | pad | bytes 2162692 | tf_op jit(solution)/shard_map/pad | solution.py:44
  551.0 3.2 add.201
  554.3 31.2 %pad.56 = f32[8,128,704]{2,0,1:T(8,128)} pad(f32[8,64,704]{2,0,1:T(8,128)} %add.201, f32[]{:T(128)} %constant.10.clone.1), padding=0_0_0x1_0_1x0_0_0 | pad | bytes 4325380 | tf_op jit(solution)/shard_map/pad | solution.py:44
  585.5 3.3 copy.68
  588.8 3.4 copy.63
  592.2 1.0 copy.62
  593.3 3.2 fusion.19
  596.5 1.3 pad_maximum_fusion
  597.7 31.5 %pad.55 = f32[8,128,704]{2,0,1:T(8,128)} pad(f32[8,64,704]{2,0,1:T(8,128)} %pad_maximum_fusion, f32[]{:T(128)} %constant.10.clone.1), padding=0_0_0x0_1_1x0_0_0 | pad | bytes 4325380 | tf_op jit(solution)/shard_map/pad | solution.py:44
  629.3 4.0 add.203
  633.3 2.6 copy.58
  636.0 12.7 %convolution_convert_fusion.1 = bf16[1024,2048]{1,0:T(8,128)(2,1)} fusion(bf16[704,2048]{1,0:T(8,128)(2,1)} %all-gather.15.cloned.1.call-done, f32[88,8,8,128]{3,2,1,0:T(8,128)S(1)} %bitcast.109, bf16[2048,704]{0,1:T(8,128)(2,1)} %all-gather.13.cloned.1.call-done, bf16[1024,2048]{1,0:T(8,128)(2,1)} %all-gather.9.cloned.1.call-done, ...), kind=kOutput, calls=%fused_computation.14 | convolution fusion | flops 5923274752 | bytes 17051648 | tf_op jit(solution)/shard_map/dot_general | solution.py:62
  648.8 42.7 %reduce-scatter.3.cloned.1.call-done = bf16[1024,512]{1,0:T(8,128)(2,1)} async-done(((bf16[1024,2048]{1,0:T(8,128)(2,1)}), bf16[1024,512]{1,0:T(8,128)(2,1)}) %reduce-scatter.3.cloned.1.call-update) | async-done | bytes 1048592 | tf_op jit(solution)/shard_map/reduce_scatter | solution.py:130
  691.5 2.5 add_convert_fusion.2
  696.3 32.3 %all-gather.17.cloned.1.call-done = bf16[1024,2048]{1,0:T(8,128)(2,1)} async-done(((bf16[1024,512]{1,0:T(8,128)(2,1)}), bf16[1024,2048]{1,0:T(8,128)(2,1)}) %all-gather.17.cloned.1.call-update) | async-done | bytes 4194320 | tf_op jit(solution)/shard_map/all_gather | solution.py:134
  728.6 3.1 fusion.3
  731.7 91.4 %all-gather.19.cloned.1.call-done = bf16[2048,1408]{1,0:T(8,128)(2,1)} async-done(((bf16[256,1408]{1,0:T(8,128)(2,1)}), bf16[2048,1408]{1,0:T(8,128)(2,1)}) %all-gather.19.cloned.1.call-update) | async-done | bytes 5767184 | tf_op jit(solution)/shard_map/all_gather | solution.py:114
  823.1 12.1 %fusion.32 = f32[1024,1408]{1,0:T(8,128)} fusion(bf16[2048,1408]{1,0:T(8,128)(2,1)} %all-gather.19.cloned.1.call-done, bf16[1024,2048]{1,0:T(8,128)(2,1)} %all-gather.17.cloned.1.call-done, f32[2048]{0:T(1024)S(1)} %copy-done.18, f32[1024]{0:T(1024)S(1)} %add_rsqrt_fusion), kind=kOutput, calls=%fused_computation.53 | convolution fusion | flops 5913968640 | bytes 15740928 | tf_op jit(solution)/shard_map/dot_general | solution.py:56
  835.2 80.6 %all-gather.21.cloned.1.call-done = bf16[2048,1408]{1,0:T(8,128)(2,1)} async-done(((bf16[256,1408]{1,0:T(8,128)(2,1)}), bf16[2048,1408]{1,0:T(8,128)(2,1)}) %all-gather.21.cloned.1.call-update) | async-done | bytes 5767184 | tf_op jit(solution)/shard_map/all_gather | solution.py:115
  915.8 93.4 %all-gather.23.cloned.1.call-done = bf16[1408,2048]{1,0:T(8,128)(2,1)} async-done(((bf16[1408,256]{1,0:T(8,128)(2,1)}), bf16[1408,2048]{1,0:T(8,128)(2,1)}) %all-gather.23.cloned.1.call-update) | async-done | bytes 5767184 | tf_op jit(solution)/shard_map/all_gather | solution.py:63
  1009.2 20.9 %convolution_convert_fusion = bf16[1024,2048]{1,0:T(8,128)(2,1)} fusion(bf16[1408,2048]{1,0:T(8,128)(2,1)} %all-gather.23.cloned.1.call-done, f32[1024,1408]{1,0:T(8,128)} %fusion.32, bf16[2048,1408]{1,0:T(8,128)(2,1)} %all-gather.21.cloned.1.call-done, bf16[1024,2048]{1,0:T(8,128)(2,1)} %all-gather.17.cloned.1.call-done, f32[2048]{0:T(1024)S(1)} %copy-done.18, ...), kind=kOutput, calls=%fused_computation.13 | convolution fusion | flops 11830296576 | bytes 25702400 | tf_op jit(solution)/shard_map/dot_general | solution.py:62
  1030.1 42.7 %reduce-scatter.5.cloned.1.call-done = bf16[1024,512]{1,0:T(8,128)(2,1)} async-done(((bf16[1024,2048]{1,0:T(8,128)(2,1)}), bf16[1024,512]{1,0:T(8,128)(2,1)}) %reduce-scatter.5.cloned.1.call-update) | async-done | bytes 1048592 | tf_op jit(solution)/shard_map/reduce_scatter | solution.py:139
  1072.9 2.5 add_convert_fusion.1
  (92 shorter events, 15.2 us)
Async XLA Ops:
  6.5 39.6 %all-gather.9.cloned.1.call-start = ((), (), s32[]{:S(2)}) async-start(), calls=%async_computation.2 | async-start | bytes 5242880 | tf_op jit(solution)/shard_map/all_gather | solution.py:117
  7.3 100.5 %all-gather.11.cloned.1.call-start = ((), (), s32[]{:S(2)}) async-start(), calls=%async_computation.3 | async-start | bytes 3244032 | tf_op jit(solution)/shard_map/all_gather | solution.py:113
  8.0 628.0 %all-gather.13.cloned.1.call-start = ((), (), s32[]{:S(2)}) async-start(), calls=%async_computation.4 | async-start | bytes 3244032 | tf_op jit(solution)/shard_map/all_gather | solution.py:112
  8.7 5.8 copy-start.15
  8.8 627.2 %all-gather.15.cloned.1.call-start = ((), (), s32[]{:S(2)}) async-start(), calls=%async_computation.5 | async-start | bytes 3244032 | tf_op jit(solution)/shard_map/all_gather | solution.py:63
  9.3 682.2 %reduce-scatter.3.cloned.1.call-start = ((), (), s32[]{:S(2)}) async-start(), calls=%async_computation.6 | async-start | bytes 5242880 | tf_op jit(solution)/shard_map/reduce_scatter | solution.py:130
  14.6 93.2 %copy-start.16 = (f32[2048]{0:T(1024)S(1)}, f32[2048]{0:T(1024)}, u32[]{:S(2)}) copy-start(f32[2048]{0:T(1024)} %param.15) | copy-start | bytes 24580
  125.2 1.7 copy-start.19
  128.6 5.0 copy-start.7
  475.4 1.1 copy-start.1
  475.4 1.7 copy-start.2
  476.2 1.0 copy-start.4
  476.3 1.6 copy-start.5
  477.0 0.8 copy-start.8
  477.9 0.7 copy-start.9
  477.9 0.7 copy-start.10
  478.8 0.6 copy-start.11
  479.4 0.6 copy-start.12
  480.1 10.6 copy-start.13
  513.5 4.4 copy-start.14
  597.7 31.5 %copy-start = (f32[8,128,704]{2,0,1:T(8,128)S(1)}, f32[8,128,704]{2,0,1:T(8,128)}, u32[]{:S(2)}) copy-start(f32[8,128,704]{2,0,1:T(8,128)} %pad.56) | copy-start | bytes 8650756
  633.3 2.7 copy-start.17
  648.7 42.8 %copy-start.6 = (bf16[1024,512]{1,0:T(8,128)(2,1)S(1)}, bf16[1024,512]{1,0:T(8,128)(2,1)}, u32[]{:S(2)}) copy-start(bf16[1024,512]{1,0:T(8,128)(2,1)} %param.14) | copy-start | bytes 3145732
  648.7 79.9 %all-gather.17.cloned.1.call-start = ((), (), s32[]{:S(2)}) async-start(), calls=%async_computation.7 | async-start | bytes 5242880 | tf_op jit(solution)/shard_map/all_gather | solution.py:134
  694.0 129.1 %all-gather.19.cloned.1.call-start = ((), (), s32[]{:S(2)}) async-start(), calls=%async_computation.8 | async-start | bytes 6488064 | tf_op jit(solution)/shard_map/all_gather | solution.py:114
  694.7 128.4 %copy-start.18 = (f32[2048]{0:T(1024)S(1)}, f32[2048]{0:T(1024)}, u32[]{:S(2)}) copy-start(f32[2048]{0:T(1024)} %param.24) | copy-start | bytes 24580
  694.8 221.1 %all-gather.21.cloned.1.call-start = ((), (), s32[]{:S(2)}) async-start(), calls=%async_computation.9 | async-start | bytes 6488064 | tf_op jit(solution)/shard_map/all_gather | solution.py:115
  695.5 313.7 %all-gather.23.cloned.1.call-start = ((), (), s32[]{:S(2)}) async-start(), calls=%async_computation.10 | async-start | bytes 6488064 | tf_op jit(solution)/shard_map/all_gather | solution.py:63
  696.2 376.6 %reduce-scatter.5.cloned.1.call-start = ((), (), s32[]{:S(2)}) async-start(), calls=%async_computation.11 | async-start | bytes 5242880 | tf_op jit(solution)/shard_map/reduce_scatter | solution.py:139
  1030.1 42.8 %copy-start.3 = (bf16[1024,512]{1,0:T(8,128)(2,1)S(1)}, bf16[1024,512]{1,0:T(8,128)(2,1)}, u32[]{:S(2)}) copy-start(bf16[1024,512]{1,0:T(8,128)(2,1)} %add_convert_fusion.2) | copy-start | bytes 3145732
Sparse Core Ops, SparseCore 0:
  8.9 37.1 all-gather.8
  48.1 59.5 all-gather.10
  109.8 57.8 all-gather.12
  169.6 57.7 all-gather.14
  648.9 42.5 reduce-scatter.2
  694.1 34.4 all-gather.16
  730.8 92.2 all-gather.18
  825.3 90.4 all-gather.20
  917.9 91.2 all-gather.22
  1030.3 42.5 reduce-scatter.4
where the time goes:
time: 1100 us; the launch traced here: 1080 us
  local copies, waits for them, and re-layouts  483 us (44%)
  waiting for transfers between devices  477 us (43%)
  matrix products  60.6 us (6%)
  other arithmetic  46.9 us (4%)
  between operations  14.2 us (1%)
    slice x10, local copies, waits for them, and re-layouts, linear_scan(): result = lax.associative_scan(combine_steps, shaped, axis=1)  322 us
    pad x12, local copies, waits for them, and re-layouts, linear_scan(): result = lax.associative_scan(combine_steps, shaped, axis=1)  120 us
    all_gather x2, waiting for transfers between devices, project_down(): lax.all_gather(weight, 'fs', axis=1, tiled=True)  93.4 us
    all_gather x1, waiting for transfers between devices, shards(): lax.all_gather(feedforward_gate_weight, 'fs', axis=0, tiled=True)  91.4 us
    all_gather x1, waiting for transfers between devices, shards(): lax.all_gather(feedforward_up_weight, 'fs', axis=0, tiled=True)  80.6 us
    all_gather x1, waiting for transfers between devices, shards(): lax.all_gather(recurrence_input_weight, 'fs', axis=0, tiled=True)  58.5 us
    reduce_scatter x1, waiting for transfers between devices, shards(): lax.psum_scatter(down_term.astype(jnp.bfloat16), 'tp', scatter_dimension=...  42.7 us
    reduce_scatter x1, waiting for transfers between devices, shards(): lax.psum_scatter(mixer_term.astype(jnp.bfloat16), 'tp', scatter_dimension...  42.7 us
  transfers between devices with their start and end apart: 10, of which 8 were waited for; matrix products, arithmetic and copies ran while one was open for 51% of the time, Pallas kernels for 0%

commit v1 on v0

v1 whole, which is shorter than its diff:
```python
import jax
import jax.numpy as jnp
from jax import lax
from jax.experimental import pallas as pl
from jax.experimental.pallas import tpu as pltpu
from jax.sharding import PartitionSpec as P

LEN = 128
EPSILON = 1e-06
GATE_EXPONENT = 8.0
BF = jnp.bfloat16
F32 = jnp.float32


def params(*semantics):
    return pltpu.CompilerParams(dimension_semantics=semantics, vmem_limit_bytes=48 * 1024 * 1024)


def norm_kernel(place_ref, gain_ref, *refs):
    count = gain_ref.shape[0]
    pieces, out_ref = refs[:-1], refs[-1]
    width = gain_ref.shape[2]
    for group in range(len(pieces) // count):
        own = [ref[...].astype(F32) for ref in pieces[group * count : (group + 1) * count]]
        total = jnp.sum(own[0] * own[0], axis=-1, keepdims=True)
        for piece in own[1:]:
            total = total + jnp.sum(piece * piece, axis=-1, keepdims=True)
        scale = lax.rsqrt(total * (1.0 / (count * width)) + EPSILON)
        for here in range(count):

            @pl.when(place_ref[0] == here)
            def _():
                for step in range(count):
                    at = here ^ step
                    out_ref[group, :, at * width : (at + 1) * width] = (
                        own[step] * scale * gain_ref[at]
                    ).astype(BF)


def norm_pieces(pieces, gain, place, count):
    rows, width = pieces[0].shape
    groups = len(pieces) // count
    block = min(128, rows)
    gains = gain.reshape(count, 1, width)
    out = pl.pallas_call(
        norm_kernel,
        grid=(rows // block,),
        in_specs=[
            pl.BlockSpec(memory_space=pltpu.SMEM),
            pl.BlockSpec((count, 1, width), lambda i: (0, 0, 0)),
        ]
        + [pl.BlockSpec((block, width), lambda i: (i, 0))] * len(pieces),
        out_specs=pl.BlockSpec((groups, block, count * width), lambda i: (0, i, 0)),
        out_shape=jax.ShapeDtypeStruct((groups, rows, count * width), BF),
        compiler_params=params("arbitrary"),
        name="norm_pieces",
    )(place, gains, *pieces)
    return out.reshape(groups * rows, count * width)


def recurrence_kernel(
    sequences, projected_ref, taps_ref, recur_ref, inject_ref, decay_ref, token_ref, out_ref, filter_ref, state_ref, a_ref, b_ref
):
    rows, channels = out_ref.shape
    taps = taps_ref.shape[0]
    history = (taps - 1) * sequences

    @pl.when(pl.program_id(1) == 0)
    def _():
        filter_ref[0:history, :] = jnp.zeros((history, channels), F32)
        state_ref[...] = jnp.zeros_like(state_ref)

    projected = projected_ref[...]
    gate = projected[:, :channels]
    filter_ref[history : history + rows, :] = projected[:, channels:].astype(BF).astype(F32)
    summed = taps_ref[0:1, :] * filter_ref[0:rows, :]
    for k in range(1, taps):
        summed = summed + taps_ref[k : k + 1, :] * filter_ref[k * sequences : k * sequences + rows, :]
    filter_ref[0:history, :] = filter_ref[rows : rows + history, :]
    mixed = summed.astype(BF)
    recur = jax.nn.sigmoid(jnp.dot(mixed, recur_ref[...], preferred_element_type=F32))
    inject = jax.nn.sigmoid(jnp.dot(mixed, inject_ref[...], preferred_element_type=F32))
    log_decay = decay_ref[...] * recur + token_ref[:, 0:1]
    decay = jnp.exp(log_decay)
    square = log_decay * log_decay
    small = log_decay * (
        1.0 - square * (1.0 / 3.0 - square * (2.0 / 15.0 - square * (17.0 / 315.0 - square * (62.0 / 2835.0))))
    )
    tangent = jnp.where(log_decay > -0.125, small, jnp.tanh(log_decay))
    a_ref[...] = decay
    b_ref[...] = jnp.sqrt(-tangent * (1.0 + decay * decay)) * (inject * mixed.astype(F32))
    state = state_ref[...]
    for step in range(rows // sequences):
        at = slice(step * sequences, (step + 1) * sequences)
        state = a_ref[at, :] * state + b_ref[at, :]
        b_ref[at, :] = state
    state_ref[...] = state
    out_ref[...] = (b_ref[...] * jax.nn.gelu(gate)).astype(BF)


def recurrence(projected, taps, recur, inject, decay, token_decay, sequences):
    rows, doubled = projected.shape
    channels = doubled // 2
    per = sequences * LEN
    block = sequences * 32
    steps = per // block
    import functools

    return pl.pallas_call(
        functools.partial(recurrence_kernel, sequences),
        grid=(rows // per, steps),
        in_specs=[
            pl.BlockSpec((block, doubled), lambda g, i: (g * steps + i, 0)),
            pl.BlockSpec(taps.shape, lambda g, i: (0, 0)),
            pl.BlockSpec(recur.shape, lambda g, i: (0, 0)),
            pl.BlockSpec(inject.shape, lambda g, i: (0, 0)),
            pl.BlockSpec((1, channels), lambda g, i: (0, 0)),
            pl.BlockSpec((block, token_decay.shape[1]), lambda g, i: (g * steps + i, 0)),
        ],
        out_specs=pl.BlockSpec((block, channels), lambda g, i: (g * steps + i, 0)),
        out_shape=jax.ShapeDtypeStruct((rows, channels), BF),
        scratch_shapes=[
            pltpu.VMEM((block + (taps.shape[0] - 1) * sequences, channels), F32),
            pltpu.VMEM((sequences, channels), F32),
            pltpu.VMEM((block, channels), F32),
            pltpu.VMEM((block, channels), F32),
        ],
        compiler_params=params("arbitrary", "arbitrary"),
        name="recurrence",
    )(projected, taps, recur, inject, decay, token_decay)


def time_major(rows_first, sequences):
    rows, width = rows_first.shape
    return rows_first.reshape(sequences, rows // sequences, width).swapaxes(0, 1).reshape(rows, width)


def sequence_major(time_first, sequences):
    rows, width = time_first.shape
    return time_first.reshape(rows // sequences, sequences, width).swapaxes(0, 1).reshape(rows, width)


def decay_columns(token_log_decay, sequences):
    ordered = token_log_decay.reshape(sequences, LEN).T.reshape(-1, 1)
    return jnp.broadcast_to(ordered, (ordered.shape[0], 128))


def block_dense(weight):
    groups, block_width, _ = weight.shape
    identity = jnp.eye(groups, dtype=BF)[:, None, :, None]
    return (weight[:, :, None, :] * identity).reshape(groups * block_width, groups * block_width)


def product(left, right):
    return jnp.dot(left, right, preferred_element_type=F32)


def plain_shards(
    tokens,
    recurrence_norm_gain,
    output_gate_weight,
    recurrence_input_weight,
    convolution_taps,
    recurrence_gate_weight,
    input_gate_weight,
    base_decay_logit,
    token_log_decay,
    recurrence_output_weight,
    feedforward_norm_gain,
    feedforward_gate_weight,
    feedforward_up_weight,
    feedforward_down_weight,
):
    sequences = tokens.shape[0] // LEN

    def rows_of(weight):
        return lax.all_gather(weight, "fs", axis=0, tiled=True)

    def columns_of(weight):
        return lax.all_gather(weight, "fs", axis=1, tiled=True)

    def normed_of(own, gain):
        widened = lax.all_gather(own, "tp", axis=1, tiled=True).astype(F32)
        scale = lax.rsqrt(jnp.mean(widened * widened, axis=-1, keepdims=True) + EPSILON)
        return (widened * scale * gain).astype(BF)

    def scattered(term):
        return lax.psum_scatter(term.astype(BF), "tp", scatter_dimension=1, tiled=True).astype(F32)

    ordered = time_major(tokens, sequences)
    normed = normed_of(ordered, recurrence_norm_gain)
    projected = jnp.concatenate(
        [product(normed, rows_of(output_gate_weight)), product(normed, rows_of(recurrence_input_weight))], axis=1
    )
    carried = recurrence(
        projected,
        convolution_taps,
        block_dense(recurrence_gate_weight),
        block_dense(input_gate_weight),
        -GATE_EXPONENT * jax.nn.softplus(-base_decay_logit)[None, :],
        decay_columns(token_log_decay, sequences),
        sequences,
    )
    mixed = scattered(product(carried, columns_of(recurrence_output_weight)))
    residual = sequence_major((ordered.astype(F32) + mixed).astype(BF), sequences)
    normed_two = normed_of(residual, feedforward_norm_gain)
    gate_hidden = product(normed_two, rows_of(feedforward_gate_weight))
    up_hidden = product(normed_two, rows_of(feedforward_up_weight))
    hidden = (jax.nn.silu(gate_hidden) * up_hidden).astype(BF)
    down = scattered(product(hidden, columns_of(feedforward_down_weight)))
    return (residual.astype(F32) + down).astype(BF)


def paired_shards(
    tokens,
    recurrence_norm_gain,
    output_gate_weight,
    recurrence_input_weight,
    convolution_taps,
    recurrence_gate_weight,
    input_gate_weight,
    base_decay_logit,
    token_log_decay,
    recurrence_output_weight,
    feedforward_norm_gain,
    feedforward_gate_weight,
    feedforward_up_weight,
    feedforward_down_weight,
):
    fs, tp = lax.axis_size("fs"), lax.axis_size("tp")
    side = lax.axis_index("fs") % 2
    place = lax.axis_index("tp")
    rows = tokens.shape[0]
    sequences = rows // LEN
    first = side == 0
    lines = [[way + 2 * i for i in range(fs // 2)] for way in range(2)]

    def over_x(value):
        return lax.ppermute(value, "fs", [(i, i ^ 1) for i in range(fs)])

    def over_tp(value, bit):
        return lax.ppermute(value, "tp", [(i, i ^ bit) for i in range(tp)])

    def halves(weight, axis):
        low, high = jnp.split(weight, 2, axis=axis)
        return jnp.where(first, low, high), jnp.where(first, high, low)

    def in_order(own, other):
        return jnp.where(first, jnp.stack([own, other]), jnp.stack([other, own]))

    def gathered(own, other, axis=0):
        pair = in_order(own, over_x(other))
        out = lax.all_gather(pair, "fs", axis=0, tiled=True, axis_index_groups=lines)
        return out

    gate_own, gate_other = halves(output_gate_weight, 1)
    in_own, in_other = halves(recurrence_input_weight, 1)
    project_weight = gathered(
        jnp.concatenate([gate_own, in_own], 1), jnp.concatenate([gate_other, in_other], 1)
    )
    project_weight = project_weight.reshape(-1, project_weight.shape[-1])
    out_weight = gathered(*halves(recurrence_output_weight, 0))
    ffn_gate_own, ffn_gate_other = halves(feedforward_gate_weight, 1)
    ffn_up_own, ffn_up_other = halves(feedforward_up_weight, 1)
    ffn_pair = in_order(
        jnp.stack([ffn_gate_own, ffn_up_own]), over_x(jnp.stack([ffn_gate_other, ffn_up_other]))
    )
    ffn_pair = ffn_pair.swapaxes(0, 1).reshape(2, -1, ffn_gate_own.shape[-1])
    ffn_weight = lax.all_gather(ffn_pair, "fs", axis=1, tiled=True, axis_index_groups=lines)
    down_weight = gathered(*halves(feedforward_down_weight, 0))

    def spread(own):
        half = rows // 2
        over, across = over_x(own), over_tp(own, 2)
        corner = jnp.concatenate([over_tp(over[:half], 2), over_x(across[half:])], axis=0)
        return [
            own, over_tp(own, 1), across, over_tp(across, 1),
            over, over_tp(over, 1), corner, over_tp(corner, 1),
        ]

    def columns(weight, step):
        each = weight.shape[0] // tp
        chosen = lax.dynamic_slice_in_dim(weight, (place ^ step) * each, each, axis=0)
        return chosen.swapaxes(0, 1).reshape(weight.shape[1], -1)

    def summed_to_owner(values, weight):
        half = rows // 2
        part = {step: product(values, columns(weight, step)).astype(BF) for step in (3, 1, 2, 0)}
        far = part[2].astype(F32) + over_tp(part[3], 1).astype(F32)
        near = part[0].astype(F32) + over_tp(part[1], 1).astype(F32)
        corner = far[rows:].astype(BF)
        by_x, by_y = over_x(corner[:half]), over_tp(corner[half:], 2)
        to_y = jnp.concatenate([far[:half] + by_x.astype(F32), far[half:rows]], axis=0)
        to_x = jnp.concatenate([near[rows : rows + half], near[rows + half :] + by_y.astype(F32)], axis=0)
        from_y, from_x = over_tp(to_y.astype(BF), 2), over_x(to_x.astype(BF))
        return near[:rows] + from_y.astype(F32) + from_x.astype(F32)

    places = place.reshape(1).astype(jnp.int32)
    ordered = time_major(tokens, sequences)
    normed = norm_pieces(spread(ordered), recurrence_norm_gain, places, tp)
    projected = product(normed, project_weight)
    token_decay = token_log_decay.reshape(sequences, LEN)
    token_columns = jnp.concatenate(
        [decay_columns(token_decay, sequences), decay_columns(over_x(token_decay), sequences)], axis=0
    )
    carried = recurrence(
        projected,
        halves(convolution_taps, 1)[0],
        block_dense(halves(recurrence_gate_weight, 0)[0]),
        block_dense(halves(input_gate_weight, 0)[0]),
        -GATE_EXPONENT * jax.nn.softplus(-halves(base_decay_logit, 0)[0])[None, :],
        token_columns,
        sequences,
    )
    mixed = summed_to_owner(carried, out_weight)
    residual = sequence_major((ordered.astype(F32) + mixed).astype(BF), sequences)
    normed_two = norm_pieces(spread(residual), feedforward_norm_gain, places, tp)
    hidden = (jax.nn.silu(product(normed_two, ffn_weight[0])) * product(normed_two, ffn_weight[1])).astype(BF)
    down = summed_to_owner(hidden, down_weight)
    return (residual.astype(F32) + down).astype(BF)


def solution(mesh):
    in_specs = (
        P("fs", "tp"), P(), P("fs", "tp"), P("fs", "tp"), P(None, "tp"), P("tp", None, None), P("tp", None, None),
        P("tp"), P("fs"), P("tp", "fs"), P(), P("fs", "tp"), P("fs", "tp"), P("tp", "fs"),
    )
    fs, tp = mesh.shape["fs"], mesh.shape["tp"]

    def whole(*args):
        blocks = args[5].shape[0] // tp
        paired = fs % 2 == 0 and tp == 4 and blocks % 2 == 0
        body = paired_shards if paired else plain_shards
        return jax.shard_map(
            body, mesh=mesh, in_specs=in_specs, out_specs=P("fs", "tp"), check_vma=False
        )(*args)

    return whole
```

time: 1100 us -> 353 us (0.32); the launches traced: 1080 us -> 352 us
  local copies, waits for them, and re-layouts: 483 us -> 29.7 us
  waiting for transfers between devices: 477 us -> 190 us
  Pallas kernels: 0 us -> 30.3 us
  starting transfers between devices: 0.35 us -> 29.4 us
  other arithmetic: 46.9 us -> 18.3 us
  matrix products: 60.6 us -> 40.1 us
    all_gather x8 -> x4, waiting for transfers between devices: 387 us -> 41.2 us  [the longest x1 41.2 us: paired_shards(): lax.all_gather(ffn_pair, 'fs', axis=1, tiled=True, axis_index_groups=lines)]
    slice x15 -> x8, local copies, waits for them, and re-layouts: 330 us -> 1.27 us  [the longest x2 0.86 us: spread(): over[:half]]
    ppermute x0 -> x33, waiting for transfers between devices: none -> 149 us  [the longest x13 92 us: over_x(): return lax.ppermute(value, 'fs', [(i, i ^ 1) for i in range(fs)])]
    pad x12 -> x0, local copies, waits for them, and re-layouts: 120 us -> none  [linear_scan(): result = lax.associative_scan(combine_steps, shaped, axis=1)]
    reduce_scatter x2 -> x0, waiting for transfers between devices: 85.4 us -> none  [the longest x1 42.7 us: shards(): lax.psum_scatter(down_term.astype(jnp.bfloat16), 'tp', scatter_dimension=...]
    pallas_call x0 -> x3, Pallas kernels: none -> 30.3 us  [the longest x2 20.5 us: norm_pieces(): pl.pallas_call(norm_kernel, grid=(rows // block,), in_specs=[pl.BlockSpec...]
    ppermute x0 -> x33, starting transfers between devices: none -> 29.2 us  [the longest x13 17.1 us: over_x(): return lax.ppermute(value, 'fs', [(i, i ^ 1) for i in range(fs)])]
    add x13 -> x0, other arithmetic: 22.2 us -> none  [the longest x7 13.7 us: linear_scan(): result = lax.associative_scan(combine_steps, shaped, axis=1)]
  transfers between devices with their start and end apart: 10 -> 37, of which waited for: 8 -> 18; matrix products, arithmetic and copies ran while one was open for 51% -> 19% of each run, Pallas kernels for 0% -> 9%
where the time goes in v1:
time: 353 us; the launch traced here: 352 us
  waiting for transfers between devices  190 us (54%)
  matrix products  40.1 us (11%)
  Pallas kernels  30.3 us (9%)
  local copies, waits for them, and re-layouts  29.7 us (8%)
  starting transfers between devices  29.4 us (8%)
  other arithmetic  18.3 us (5%)
  between operations  13.7 us (4%)
    ppermute x13, waiting for transfers between devices, over_x(): return lax.ppermute(value, 'fs', [(i, i ^ 1) for i in range(fs)])  92 us
    ppermute x20, waiting for transfers between devices, over_tp(): return lax.ppermute(value, 'tp', [(i, i ^ bit) for i in range(tp)])  57 us
    all_gather x1, waiting for transfers between devices, paired_shards(): lax.all_gather(ffn_pair, 'fs', axis=1, tiled=True, axis_index_groups=lines)  41.2 us
    dot_general x11, matrix products, product(): return jnp.dot(left, right, preferred_element_type=F32)  40.1 us
    pallas_call x2, Pallas kernels, norm_pieces(): pl.pallas_call(norm_kernel, grid=(rows // block,), in_specs=[pl.BlockSpec...  20.5 us
    ppermute x13, starting transfers between devices, over_x(): return lax.ppermute(value, 'fs', [(i, i ^ 1) for i in range(fs)])  17.1 us
    unnamed x48, local copies, waits for them, and re-layouts  14.2 us
    ppermute x20, starting transfers between devices, over_tp(): return lax.ppermute(value, 'tp', [(i, i ^ bit) for i in range(tp)])  12.1 us
  transfers between devices with their start and end apart: 37, of which 18 were waited for; matrix products, arithmetic and copies ran while one was open for 19% of the time, Pallas kernels for 9%

profile of v1, /device:TPU:0, one launch (start us, length us, event | category | flops | bytes accessed | tf_op | source)
XLA Modules:
  0.0 351.8 jit_solution(11857817275239647306)
XLA Ops:
  6.5 1.0 select_bitcast_fusion.7
  7.6 3.0 collective-permute-start.10
  10.6 4.5 %collective-permute-done.10 = bf16[352,256]{1,0:T(8,128)(2,1)S(1)} collective-permute-done((bf16[352,256]{1,0:T(8,128)(2,1)S(1)}, bf16[352,256]{1,0:T(8,128)(2,1)S(1)}, u32[]{:S(2)}, u32[]{:S(2)}) %collective-permute-start.10) | collective-permute-done | bytes 180256 | tf_op jit(solution)/shard_map/ppermute | solution.py:239
  16.0 1.3 broadcast_select_fusion.4
  17.4 1.8 collective-permute-start.8
  19.2 7.8 %collective-permute-done.8 = bf16[256,704]{0,1:T(8,128)(2,1)S(1)} collective-permute-done((bf16[256,704]{0,1:T(8,128)(2,1)S(1)}, bf16[256,704]{0,1:T(8,128)(2,1)S(1)}, u32[]{:S(2)}, u32[]{:S(2)}) %collective-permute-start.8) | collective-permute-done | bytes 360480 | tf_op jit(solution)/shard_map/ppermute | solution.py:239
  28.2 1.5 collective-permute-start.26
  29.7 7.3 %collective-permute-done.26 = bf16[704,256]{1,0:T(8,128)(2,1)S(1)} collective-permute-done((bf16[704,256]{1,0:T(8,128)(2,1)S(1)}, bf16[704,256]{1,0:T(8,128)(2,1)S(1)}, u32[]{:S(2)}, u32[]{:S(2)}) %collective-permute-start.26) | collective-permute-done | bytes 360480 | tf_op jit(solution)/shard_map/ppermute | solution.py:239
  36.9 1.0 maximum_select_fusion.2
  38.6 1.2 collective-permute-start.3
  39.9 1.5 collective-permute-start.1
  41.9 2.0 fusion.17
  43.9 17.5 %collective-permute-done.3.refs_4_ = bf16[1024,512]{1,0:T(8,128)(2,1)S(1)} collective-permute-done((bf16[1024,512]{1,0:T(8,128)(2,1)S(1)}, bf16[1024,512]{1,0:T(8,128)(2,1)S(1)}, u32[]{:S(2)}, u32[]{:S(2)}) %collective-permute-start.3) | collective-permute-done | bytes 1048608 | tf_op jit(solution)/shard_map/ppermute | solution.py:239
  63.2 2.1 fusion.18
  65.3 1.9 copy.66
  68.1 1.2 copy.68
  69.3 1.9 copy.69
  71.3 1.6 collective-permute-start.6
  72.8 2.2 select_bitcast_fusion.3
  76.5 1.9 constant_dynamic-update-slice_fusion.1
  78.4 7.8 %collective-permute-done.6 = bf16[512,512]{1,0:T(8,128)(2,1)S(1)} collective-permute-done((bf16[512,512]{1,0:T(8,128)(2,1)S(1)}, bf16[512,512]{1,0:T(8,128)(2,1)S(1)}, u32[]{:S(2)}, u32[]{:S(2)}) %collective-permute-start.6) | collective-permute-done | bytes 524320 | tf_op jit(solution)/shard_map/ppermute | solution.py:239
  89.3 2.0 maximum_bitcast_fusion
  91.3 2.0 select_bitcast_fusion.5
  93.5 3.6 %collective-permute-done.25 = bf16[2,256,704]{1,2,0:T(8,128)(2,1)} collective-permute-done((bf16[2,256,704]{1,2,0:T(8,128)(2,1)}, bf16[2,256,704]{1,2,0:T(8,128)(2,1)}, u32[]{:S(2)}, u32[]{:S(2)}) %collective-permute-start.25) | collective-permute-done | bytes 720928 | tf_op jit(solution)/shard_map/ppermute | solution.py:239
  97.0 2.2 fusion.8
  99.2 1.3 copy.75
  100.6 2.4 dynamic-slice_bitcast_fusion.5
  103.7 10.2 %norm_pieces.2 = bf16[2,1024,2048]{2,1,0:T(8,128)(2,1)} custom-call(s32[1]{0:T(128)} %bitcast.3.place_ref, f32[4,1,512]{2,1,0:T(1,128)S(1)} %bitcast.121, bf16[1024,512]{1,0:T(8,128)(2,1)S(1)} %bitcast.120, bf16[1024,512]{1,0:T(8,128)(2,1)} %collective-permute-done.refs_1_, bf16[1024,512]{1,0:T(8,128)(2,1)S(1)} %collective-permute-done.1.refs_2_, ...), custom_call_target="tpu_custom_call" | custom-call | tf_op jit(solution)/shard_map/norm_pieces/pallas_call | solution.py:45
  113.9 2.2 copy.70
  116.1 10.8 %fusion.21.projected_ref = f32[2048,704]{1,0:T(8,128)} fusion(bf16[2048,2048]{1,0:T(8,128)(2,1)} %bitcast.123, bf16[2048,704]{0,1:T(8,128)(2,1)S(1)} %bitcast.130), kind=kOutput, calls=%fused_computation.86 | convolution fusion | flops 5905580032 | bytes 17039360 | tf_op jit(solution)/shard_map/dot_general | solution.py:155
  127.3 9.8 %recurrence.1 = bf16[2048,352]{1,0:T(8,128)(2,1)S(1)} custom-call(f32[2048,704]{1,0:T(8,128)} %fusion.21.projected_ref, f32[4,352]{1,0:T(4,128)S(1)} %slice_select_fusion.taps_ref, bf16[352,352]{1,0:T(8,128)(2,1)S(1)} %copy-done, bf16[352,352]{1,0:T(8,128)(2,1)S(1)} %get-tuple-element.41.inject_ref, f32[1,352]{1,0:T(1,128)S(1)} %mul.33.decay_ref, ...), custom_call_target="tpu_custom_call" | custom-call | tf_op jit(solution)/shard_map/recurrence/pallas_call | solution.py:109
  137.1 1.2 convolution_convert_fusion.4
  138.5 1.3 convolution_convert_fusion.6
  140.3 2.3 collective-permute-done.12
  142.6 1.3 fusion.19
  144.0 1.5 collective-permute-start.13
  146.3 1.3 convert_add_fusion.3
  147.6 10.4 %collective-permute-done.13 = bf16[512,512]{1,0:T(8,128)(2,1)S(1)} collective-permute-done((bf16[512,512]{1,0:T(8,128)(2,1)S(1)}, bf16[512,512]{1,0:T(8,128)(2,1)S(1)}, u32[]{:S(2)}, u32[]{:S(2)}) %collective-permute-start.13) | collective-permute-done | bytes 524320 | tf_op jit(solution)/shard_map/ppermute | solution.py:239
  158.3 1.4 collective-permute-start.14
  160.7 22.1 %collective-permute-done.14 = bf16[1024,512]{1,0:T(8,128)(2,1)S(1)} collective-permute-done((bf16[1024,512]{1,0:T(8,128)(2,1)S(1)}, bf16[1024,512]{1,0:T(8,128)(2,1)S(1)}, u32[]{:S(2)}, u32[]{:S(2)}) %collective-permute-start.14) | collective-permute-done | bytes 1048608 | tf_op jit(solution)/shard_map/ppermute | solution.py:242
  182.8 1.4 collective-permute-done.16
  185.5 1.0 collective-permute-start.20
  186.5 1.2 collective-permute-start.18
  187.7 21.2 %collective-permute-done.20.refs_4_ = bf16[1024,512]{1,0:T(8,128)(2,1)S(1)} collective-permute-done((bf16[1024,512]{1,0:T(8,128)(2,1)S(1)}, bf16[1024,512]{1,0:T(8,128)(2,1)S(1)}, u32[]{:S(2)}, u32[]{:S(2)}) %collective-permute-start.20) | collective-permute-done | bytes 1048608 | tf_op jit(solution)/shard_map/ppermute | solution.py:239
  208.9 1.1 collective-permute-start.22
  211.7 9.3 %collective-permute-done.22 = bf16[512,512]{1,0:T(8,128)(2,1)S(1)} collective-permute-done((bf16[512,512]{1,0:T(8,128)(2,1)S(1)}, bf16[512,512]{1,0:T(8,128)(2,1)S(1)}, u32[]{:S(2)}, u32[]{:S(2)}) %collective-permute-start.22) | collective-permute-done | bytes 524320 | tf_op jit(solution)/shard_map/ppermute | solution.py:242
  222.7 3.2 dynamic-slice_bitcast_fusion.1
  226.9 10.3 %norm_pieces.3 = bf16[2,1024,2048]{2,1,0:T(8,128)(2,1)} custom-call(s32[1]{0:T(128)} %bitcast.3.place_ref, f32[4,1,512]{2,1,0:T(1,128)S(1)} %bitcast.122, bf16[1024,512]{1,0:T(8,128)(2,1)S(1)} %bitcast.116, bf16[1024,512]{1,0:T(8,128)(2,1)} %collective-permute-done.17.refs_1_, bf16[1024,512]{1,0:T(8,128)(2,1)S(1)} %collective-permute-done.18.refs_2_, ...), custom_call_target="tpu_custom_call" | custom-call | tf_op jit(solution)/shard_map/norm_pieces/pallas_call | solution.py:45
  237.2 41.2 %all-gather.9.cloned.1.call-done = bf16[2,2048,704]{1,2,0:T(8,128)(2,1)} async-done(((bf16[2,512,704]{1,2,0:T(8,128)(2,1)}), bf16[2,2048,704]{1,2,0:T(8,128)(2,1)}) %all-gather.9.cloned.1.call-update) | async-done | bytes 5767184 | tf_op jit(solution)/shard_map/all_gather | solution.py:269
  278.3 9.6 %fusion.1 = f32[2048,704]{0,1:T(8,128)S(1)} fusion(bf16[2048,2048]{1,0:T(8,128)(2,1)} %bitcast.124, bf16[2,2048,704]{1,2,0:T(8,128)(2,1)} %all-gather.9.cloned.1.call-done), kind=kOutput, calls=%fused_computation.16 | convolution fusion | flops 5905580032 | bytes 17039360 | tf_op jit(solution)/shard_map/dot_general | solution.py:155
  288.0 7.3 %multiply_convert_fusion = bf16[2048,704]{0,1:T(8,128)(2,1)S(1)} fusion(f32[2048,704]{0,1:T(8,128)S(1)} %fusion.1, bf16[2048,2048]{1,0:T(8,128)(2,1)S(1)} %bitcast.125, bf16[2,2048,704]{1,2,0:T(8,128)(2,1)S(1)} %copy-done.19), kind=kOutput, calls=%fused_computation | convolution fusion | flops 5914230784 | bytes 19922944 | tf_op jit(solution)/shard_map/dot_general | solution.py:155
  295.3 1.9 convolution_convert_fusion
  297.3 1.9 convolution_convert_fusion.2
  299.9 1.5 collective-permute-done.28
  301.4 1.8 fusion.20
  303.3 1.5 collective-permute-start.29
  304.9 1.5 collective-permute-start.31
  306.3 1.8 convert_add_fusion.1
  308.3 9.1 %collective-permute-done.29 = bf16[512,512]{1,0:T(8,128)(2,1)S(1)} collective-permute-done((bf16[512,512]{1,0:T(8,128)(2,1)S(1)}, bf16[512,512]{1,0:T(8,128)(2,1)S(1)}, u32[]{:S(2)}, u32[]{:S(2)}) %collective-permute-start.29) | collective-permute-done | bytes 524320 | tf_op jit(solution)/shard_map/ppermute | solution.py:239
  317.6 1.5 collective-permute-start.30
  319.5 1.5 collective-permute-start.32
  321.0 21.1 %collective-permute-done.30 = bf16[1024,512]{1,0:T(8,128)(2,1)S(1)} collective-permute-done((bf16[1024,512]{1,0:T(8,128)(2,1)S(1)}, bf16[1024,512]{1,0:T(8,128)(2,1)S(1)}, u32[]{:S(2)}, u32[]{:S(2)}) %collective-permute-start.30) | collective-permute-done | bytes 1048608 | tf_op jit(solution)/shard_map/ppermute | solution.py:242
  342.1 1.5 collective-permute-done.32
  343.6 1.7 fusion.4
  (132 shorter events, 22.0 us)
Async XLA Ops:
  6.5 94.0 %all-gather.7.cloned.1.call-start = ((), (), s32[]{:S(2)}) async-start(), calls=%async_computation.1 | async-start | bytes 1802240 | tf_op jit(solution)/shard_map/all_gather | solution.py:253
  7.6 7.6 %collective-permute-start.10 = (bf16[352,256]{1,0:T(8,128)(2,1)S(1)}, bf16[352,256]{1,0:T(8,128)(2,1)S(1)}, u32[]{:S(2)}, u32[]{:S(2)}) collective-permute-start(bf16[352,256]{1,0:T(8,128)(2,1)S(1)} %get-tuple-element.30), channel_id=1, source_target_pairs={{0,4},{4,0},{8,12},{12,8},{16,20},{20,16},{24,28},{28,24},{1,5},{5... | collective-permute-start | bytes 540680 | tf_op jit(solution)/shard_map/ppermute | solution.py:239
  16.0 12.1 %copy-start.14 = (bf16[1408,256]{1,0:T(8,128)(2,1)S(1)}, bf16[1408,256]{1,0:T(8,128)(2,1)}, u32[]{:S(2)}) copy-start(bf16[1408,256]{1,0:T(8,128)(2,1)} %param.27) | copy-start | bytes 2162692
  16.0 98.0 %all-gather.5.cloned.1.call-start = ((), (), s32[]{:S(2)}) async-start(), calls=%async_computation | async-start | bytes 3604480 | tf_op jit(solution)/shard_map/all_gather | solution.py:253
  17.4 9.6 %collective-permute-start.8 = (bf16[256,704]{0,1:T(8,128)(2,1)S(1)}, bf16[256,704]{0,1:T(8,128)(2,1)S(1)}, u32[]{:S(2)}, u32[]{:S(2)}) collective-permute-start(bf16[256,704]{0,1:T(8,128)(2,1)S(1)} %pad_maximum_fusion.5), channel_id=1, source_target_pairs={{0,4},{4,0},{8,12},{12,8},{16,20},{20,16},{24,28},{28,24},{1,5},{5... | collective-permute-start | bytes 1081352 | tf_op jit(solution)/shard_map/ppermute | solution.py:239
  27.0 11.0 %copy-start.4 = (bf16[1024,512]{1,0:T(8,128)(2,1)S(1)}, bf16[1024,512]{1,0:T(8,128)(2,1)}, u32[]{:S(2)}) copy-start(bf16[1024,512]{1,0:T(8,128)(2,1)} %param.14) | copy-start | bytes 3145732
  28.0 13.4 %copy-start.17 = (f32[1024]{0:T(1024)S(1)}, f32[1024]{0:T(1024)}, u32[]{:S(2)}) copy-start(f32[1024]{0:T(1024)} %param.22) | copy-start | bytes 12292
  28.0 194.7 %all-gather.11.cloned.1.call-start = ((), (), s32[]{:S(2)}) async-start(), calls=%async_computation.3 | async-start | bytes 3604480 | tf_op jit(solution)/shard_map/all_gather | solution.py:253
  28.2 8.8 %collective-permute-start.26 = (bf16[704,256]{1,0:T(8,128)(2,1)S(1)}, bf16[704,256]{1,0:T(8,128)(2,1)S(1)}, u32[]{:S(2)}, u32[]{:S(2)}) collective-permute-start(bf16[704,256]{1,0:T(8,128)(2,1)S(1)} %get-tuple-element.20), channel_id=1, source_target_pairs={{0,4},{4,0},{8,12},{12,8},{16,20},{20,16},{24,28},{28,24},{1,5},{5... | collective-permute-start | bytes 1081352 | tf_op jit(solution)/shard_map/ppermute | solution.py:239
  38.0 240.4 %all-gather.9.cloned.1.call-start = ((), (), s32[]{:S(2)}) async-start(), calls=%async_computation.2 | async-start | bytes 7208960 | tf_op jit(solution)/shard_map/all_gather | solution.py:269
  38.6 22.8 %collective-permute-start.3 = (bf16[1024,512]{1,0:T(8,128)(2,1)S(1)}, bf16[1024,512]{1,0:T(8,128)(2,1)S(1)}, u32[]{:S(2)}, u32[]{:S(2)}) collective-permute-start(bf16[1024,512]{1,0:T(8,128)(2,1)S(1)} %bitcast.117), channel_id=1, source_target_pairs={{0,4},{4,0},{8,12},{12,8},{16,20},{20,16},{24,28},{28,24},{1,5},{5... | collective-permute-start | bytes 3145736 | tf_op jit(solution)/shard_map/ppermute | solution.py:239
  39.9 31.4 %collective-permute-start.1 = (bf16[1024,512]{1,0:T(8,128)(2,1)S(1)}, bf16[1024,512]{1,0:T(8,128)(2,1)S(1)}, u32[]{:S(2)}, u32[]{:S(2)}) collective-permute-start(bf16[1024,512]{1,0:T(8,128)(2,1)S(1)} %bitcast.118), channel_id=1, source_target_pairs={{0,2},{1,3},{2,0},{3,1},{4,6},{5,7},{6,4},{7,5},{8,10},{9,11},{10,... | collective-permute-start | bytes 3145736 | tf_op jit(solution)/shard_map/ppermute | solution.py:242
  41.4 62.3 %collective-permute-start = (bf16[1024,512]{1,0:T(8,128)(2,1)S(1)}, bf16[1024,512]{1,0:T(8,128)(2,1)}, u32[]{:S(2)}, u32[]{:S(2)}) collective-permute-start(bf16[1024,512]{1,0:T(8,128)(2,1)S(1)} %bitcast.119), channel_id=1, source_target_pairs={{0,1},{1,0},{2,3},{3,2},{4,5},{5,4},{6,7},{7,6},{8,9},{9,8},{10,11... | collective-permute-start | bytes 3145736 | tf_op jit(solution)/shard_map/ppermute | solution.py:242
  41.4 45.6 %collective-permute-start.9 = (f32[8,128]{1,0:T(8,128)S(1)}, f32[8,128]{1,0:T(8,128)S(1)}, u32[]{:S(2)}, u32[]{:S(2)}) collective-permute-start(f32[8,128]{1,0:T(8,128)S(1)} %bitcast.142), channel_id=1, source_target_pairs={{0,4},{4,0},{8,12},{12,8},{16,20},{20,16},{24,28},{28,24},{1,5},{5... | collective-permute-start | bytes 12296 | tf_op jit(solution)/shard_map/ppermute | solution.py:239
  62.3 14.2 %collective-permute-start.5 = (bf16[512,512]{1,0:T(8,128)(2,1)}, bf16[512,512]{1,0:T(8,128)(2,1)}, u32[]{:S(2)}, u32[]{:S(2)}) collective-permute-start(bf16[512,512]{1,0:T(8,128)(2,1)} %slice.92), channel_id=1, source_target_pairs={{0,2},{1,3},{2,0},{3,1},{4,6},{5,7},{6,4},{7,5},{8,10},{9,11},{10,... | collective-permute-start | bytes 1572872 | tf_op jit(solution)/shard_map/ppermute | solution.py:242
  71.3 16.2 %copy-start.18 = (f32[704]{0:T(1024)S(1)}, f32[704]{0:T(1024)}, u32[]{:S(2)}) copy-start(f32[704]{0:T(1024)} %param.21) | copy-start | bytes 8452
  71.3 14.9 %collective-permute-start.6 = (bf16[512,512]{1,0:T(8,128)(2,1)S(1)}, bf16[512,512]{1,0:T(8,128)(2,1)S(1)}, u32[]{:S(2)}, u32[]{:S(2)}) collective-permute-start(bf16[512,512]{1,0:T(8,128)(2,1)S(1)} %slice.93), channel_id=1, source_target_pairs={{0,4},{4,0},{8,12},{12,8},{16,20},{20,16},{24,28},{28,24},{1,5},{5... | collective-permute-start | bytes 1572872 | tf_op jit(solution)/shard_map/ppermute | solution.py:239
  75.0 14.2 %copy-start.12 = (bf16[1,256,704]{1,2,0:T(8,128)(2,1)S(1)}, bf16[1,256,704]{1,2,0:T(8,128)(2,1)}, u32[]{:S(2)}) copy-start(bf16[1,256,704]{1,2,0:T(8,128)(2,1)} %get-tuple-element.23) | copy-start | bytes 1081348
  75.0 16.2 %copy-start.16 = (f32[4,704]{1,0:T(4,128)S(1)}, f32[4,704]{1,0:T(4,128)}, u32[]{:S(2)}) copy-start(f32[4,704]{1,0:T(4,128)} %param.18) | copy-start | bytes 33796
  76.0 21.0 %collective-permute-start.25 = (bf16[2,256,704]{1,2,0:T(8,128)(2,1)}, bf16[2,256,704]{1,2,0:T(8,128)(2,1)}, u32[]{:S(2)}, u32[]{:S(2)}) collective-permute-start(bf16[2,256,704]{1,2,0:T(8,128)(2,1)} %pad_maximum_fusion.4), channel_id=1, source_target_pairs={{0,4},{4,0},{8,12},{12,8},{16,20},{20,16},{24,28},{28,24},{1,5},{5... | collective-permute-start | bytes 2162696 | tf_op jit(solution)/shard_map/ppermute | solution.py:239
  76.5 27.2 %collective-permute-start.2 = (bf16[1024,512]{1,0:T(8,128)(2,1)S(1)}, bf16[1024,512]{1,0:T(8,128)(2,1)}, u32[]{:S(2)}, u32[]{:S(2)}) collective-permute-start(bf16[1024,512]{1,0:T(8,128)(2,1)S(1)} %collective-permute-done.1.refs_2_), channel_id=1, source_target_pairs={{0,1},{1,0},{2,3},{3,2},{4,5},{5,4},{6,7},{7,6},{8,9},{9,8},{10,11... | collective-permute-start | bytes 3145736 | tf_op jit(solution)/shard_map/ppermute | solution.py:242
  86.1 17.5 %collective-permute-start.4 = (bf16[1024,512]{1,0:T(8,128)(2,1)S(1)}, bf16[1024,512]{1,0:T(8,128)(2,1)}, u32[]{:S(2)}, u32[]{:S(2)}) collective-permute-start(bf16[1024,512]{1,0:T(8,128)(2,1)S(1)} %collective-permute-done.3.refs_4_), channel_id=1, source_target_pairs={{0,1},{1,0},{2,3},{3,2},{4,5},{5,4},{6,7},{7,6},{8,9},{9,8},{10,11... | collective-permute-start | bytes 3145736 | tf_op jit(solution)/shard_map/ppermute | solution.py:242
  87.0 16.7 %collective-permute-start.7 = (bf16[1024,512]{1,0:T(8,128)(2,1)}, bf16[1024,512]{1,0:T(8,128)(2,1)}, u32[]{:S(2)}, u32[]{:S(2)}) collective-permute-start(bf16[1024,512]{1,0:T(8,128)(2,1)} %constant_dynamic-update-slice_fusion.refs_6_), channel_id=1, source_target_pairs={{0,1},{1,0},{2,3},{3,2},{4,5},{5,4},{6,7},{7,6},{8,9},{9,8},{10,11... | collective-permute-start | bytes 3145736 | tf_op jit(solution)/shard_map/ppermute | solution.py:242
  100.5 3.2 copy-start.1
  116.1 11.1 %copy-start = (bf16[352,352]{1,0:T(8,128)(2,1)S(1)}, bf16[352,352]{1,0:T(8,128)(2,1)}, u32[]{:S(2)}) copy-start(bf16[352,352]{1,0:T(8,128)(2,1)} %get-tuple-element.42.recur_ref) | copy-start | bytes 743428
  127.3 9.8 %copy-start.15 = (bf16[2,44,8,256]{3,2,0,1:T(8,128)(2,1)S(1)}, bf16[2,44,8,256]{3,2,0,1:T(8,128)(2,1)}, u32[]{:S(2)}) copy-start(bf16[2,44,8,256]{3,2,0,1:T(8,128)(2,1)} %copy.74) | copy-start | bytes 1081348
  137.1 1.3 copy-start.11
  138.4 4.2 %collective-permute-start.12 = (bf16[2048,512]{1,0:T(8,128)(2,1)S(1)}, bf16[2048,512]{1,0:T(8,128)(2,1)S(1)}, u32[]{:S(2)}, u32[]{:S(2)}) collective-permute-start(bf16[2048,512]{1,0:T(8,128)(2,1)S(1)} %convolution_convert_fusion.4), channel_id=1, source_target_pairs={{0,1},{1,0},{2,3},{3,2},{4,5},{5,4},{6,7},{7,6},{8,9},{9,8},{10,11... | collective-permute-start | bytes 6291464 | tf_op jit(solution)/shard_map/ppermute | solution.py:242
  138.5 1.8 copy-start.10
  139.8 6.5 %collective-permute-start.11 = (bf16[2048,512]{1,0:T(8,128)(2,1)S(1)}, bf16[2048,512]{1,0:T(8,128)(2,1)S(1)}, u32[]{:S(2)}, u32[]{:S(2)}) collective-permute-start(bf16[2048,512]{1,0:T(8,128)(2,1)S(1)} %convolution_convert_fusion.6), channel_id=1, source_target_pairs={{0,1},{1,0},{2,3},{3,2},{4,5},{5,4},{6,7},{7,6},{8,9},{9,8},{10,11... | collective-permute-start | bytes 6291464 | tf_op jit(solution)/shard_map/ppermute | solution.py:242
  143.9 1.6 copy-start.9
  144.0 14.0 %collective-permute-start.13 = (bf16[512,512]{1,0:T(8,128)(2,1)S(1)}, bf16[512,512]{1,0:T(8,128)(2,1)S(1)}, u32[]{:S(2)}, u32[]{:S(2)}) collective-permute-start(bf16[512,512]{1,0:T(8,128)(2,1)S(1)} %get-tuple-element.12), channel_id=1, source_target_pairs={{0,4},{4,0},{8,12},{12,8},{16,20},{20,16},{24,28},{28,24},{1,5},{5... | collective-permute-start | bytes 1572872 | tf_op jit(solution)/shard_map/ppermute | solution.py:239
  145.5 14.1 %collective-permute-start.15 = (bf16[512,512]{1,0:T(8,128)(2,1)S(1)}, bf16[512,512]{1,0:T(8,128)(2,1)S(1)}, u32[]{:S(2)}, u32[]{:S(2)}) collective-permute-start(bf16[512,512]{1,0:T(8,128)(2,1)S(1)} %get-tuple-element.13), channel_id=1, source_target_pairs={{0,2},{1,3},{2,0},{3,1},{4,6},{5,7},{6,4},{7,5},{8,10},{9,11},{10,... | collective-permute-start | bytes 1572872 | tf_op jit(solution)/shard_map/ppermute | solution.py:242
  158.2 26.0 %copy-start.5 = (bf16[1024,512]{1,0:T(8,128)(2,1)S(1)}, bf16[1024,512]{1,0:T(8,128)(2,1)}, u32[]{:S(2)}) copy-start(bf16[1024,512]{1,0:T(8,128)(2,1)} %param.14) | copy-start | bytes 3145732
  158.3 24.5 %collective-permute-start.14 = (bf16[1024,512]{1,0:T(8,128)(2,1)S(1)}, bf16[1024,512]{1,0:T(8,128)(2,1)S(1)}, u32[]{:S(2)}, u32[]{:S(2)}) collective-permute-start(bf16[1024,512]{1,0:T(8,128)(2,1)S(1)} %pad_maximum_fusion), channel_id=1, source_target_pairs={{0,2},{1,3},{2,0},{3,1},{4,6},{5,7},{6,4},{7,5},{8,10},{9,11},{10,... | collective-permute-start | bytes 3145736 | tf_op jit(solution)/shard_map/ppermute | solution.py:242
  159.9 24.2 %collective-permute-start.16 = (bf16[1024,512]{1,0:T(8,128)(2,1)S(1)}, bf16[1024,512]{1,0:T(8,128)(2,1)S(1)}, u32[]{:S(2)}, u32[]{:S(2)}) collective-permute-start(bf16[1024,512]{1,0:T(8,128)(2,1)S(1)} %pad_maximum_fusion.1), channel_id=1, source_target_pairs={{0,4},{4,0},{8,12},{12,8},{16,20},{20,16},{24,28},{28,24},{1,5},{5... | collective-permute-start | bytes 3145736 | tf_op jit(solution)/shard_map/ppermute | solution.py:239
  185.5 23.4 %collective-permute-start.20 = (bf16[1024,512]{1,0:T(8,128)(2,1)S(1)}, bf16[1024,512]{1,0:T(8,128)(2,1)S(1)}, u32[]{:S(2)}, u32[]{:S(2)}) collective-permute-start(bf16[1024,512]{1,0:T(8,128)(2,1)S(1)} %bitcast.113), channel_id=1, source_target_pairs={{0,4},{4,0},{8,12},{12,8},{16,20},{20,16},{24,28},{28,24},{1,5},{5... | collective-permute-start | bytes 3145736 | tf_op jit(solution)/shard_map/ppermute | solution.py:239
  186.5 24.1 %collective-permute-start.18 = (bf16[1024,512]{1,0:T(8,128)(2,1)S(1)}, bf16[1024,512]{1,0:T(8,128)(2,1)S(1)}, u32[]{:S(2)}, u32[]{:S(2)}) collective-permute-start(bf16[1024,512]{1,0:T(8,128)(2,1)S(1)} %bitcast.114), channel_id=1, source_target_pairs={{0,2},{1,3},{2,0},{3,1},{4,6},{5,7},{6,4},{7,5},{8,10},{9,11},{10,... | collective-permute-start | bytes 3145736 | tf_op jit(solution)/shard_map/ppermute | solution.py:242
  208.9 12.2 %collective-permute-start.22 = (bf16[512,512]{1,0:T(8,128)(2,1)S(1)}, bf16[512,512]{1,0:T(8,128)(2,1)S(1)}, u32[]{:S(2)}, u32[]{:S(2)}) collective-permute-start(bf16[512,512]{1,0:T(8,128)(2,1)S(1)} %slice.101), channel_id=1, source_target_pairs={{0,2},{1,3},{2,0},{3,1},{4,6},{5,7},{6,4},{7,5},{8,10},{9,11},{10,... | collective-permute-start | bytes 1572872 | tf_op jit(solution)/shard_map/ppermute | solution.py:242
  210.7 11.2 %collective-permute-start.23 = (bf16[512,512]{1,0:T(8,128)(2,1)S(1)}, bf16[512,512]{1,0:T(8,128)(2,1)S(1)}, u32[]{:S(2)}, u32[]{:S(2)}) collective-permute-start(bf16[512,512]{1,0:T(8,128)(2,1)S(1)} %slice.102), channel_id=1, source_target_pairs={{0,4},{4,0},{8,12},{12,8},{16,20},{20,16},{24,28},{28,24},{1,5},{5... | collective-permute-start | bytes 1572872 | tf_op jit(solution)/shard_map/ppermute | solution.py:239
  211.2 15.7 %collective-permute-start.17 = (bf16[1024,512]{1,0:T(8,128)(2,1)S(1)}, bf16[1024,512]{1,0:T(8,128)(2,1)}, u32[]{:S(2)}, u32[]{:S(2)}) collective-permute-start(bf16[1024,512]{1,0:T(8,128)(2,1)S(1)} %bitcast.115), channel_id=1, source_target_pairs={{0,1},{1,0},{2,3},{3,2},{4,5},{5,4},{6,7},{7,6},{8,9},{9,8},{10,11... | collective-permute-start | bytes 3145736 | tf_op jit(solution)/shard_map/ppermute | solution.py:242
  211.2 15.7 %collective-permute-start.19 = (bf16[1024,512]{1,0:T(8,128)(2,1)S(1)}, bf16[1024,512]{1,0:T(8,128)(2,1)}, u32[]{:S(2)}, u32[]{:S(2)}) collective-permute-start(bf16[1024,512]{1,0:T(8,128)(2,1)S(1)} %collective-permute-done.18.refs_2_), channel_id=1, source_target_pairs={{0,1},{1,0},{2,3},{3,2},{4,5},{5,4},{6,7},{7,6},{8,9},{9,8},{10,11... | collective-permute-start | bytes 3145736 | tf_op jit(solution)/shard_map/ppermute | solution.py:242
  211.7 15.2 %collective-permute-start.21 = (bf16[1024,512]{1,0:T(8,128)(2,1)S(1)}, bf16[1024,512]{1,0:T(8,128)(2,1)}, u32[]{:S(2)}, u32[]{:S(2)}) collective-permute-start(bf16[1024,512]{1,0:T(8,128)(2,1)S(1)} %collective-permute-done.20.refs_4_), channel_id=1, source_target_pairs={{0,1},{1,0},{2,3},{3,2},{4,5},{5,4},{6,7},{7,6},{8,9},{9,8},{10,11... | collective-permute-start | bytes 3145736 | tf_op jit(solution)/shard_map/ppermute | solution.py:242
  222.7 4.2 %copy-start.2 = (f32[2048]{0:T(1024)S(1)}, f32[2048]{0:T(1024)}, u32[]{:S(2)}) copy-start(f32[2048]{0:T(1024)} %param.24) | copy-start | bytes 24580
  222.7 4.2 %collective-permute-start.24 = (bf16[1024,512]{1,0:T(8,128)(2,1)}, bf16[1024,512]{1,0:T(8,128)(2,1)}, u32[]{:S(2)}, u32[]{:S(2)}) collective-permute-start(bf16[1024,512]{1,0:T(8,128)(2,1)} %constant_dynamic-update-slice_fusion.2.refs_6_), channel_id=1, source_target_pairs={{0,1},{1,0},{2,3},{3,2},{4,5},{5,4},{6,7},{7,6},{8,9},{9,8},{10,11... | collective-permute-start | bytes 3145736 | tf_op jit(solution)/shard_map/ppermute | solution.py:242
  278.3 9.6 %copy-start.3 = (bf16[2,1024,2048]{2,1,0:T(8,128)(2,1)S(1)}, bf16[2,1024,2048]{2,1,0:T(8,128)(2,1)}, u32[]{:S(2)}) copy-start(bf16[2,1024,2048]{2,1,0:T(8,128)(2,1)} %norm_pieces.3) | copy-start | bytes 25165828
  278.3 9.6 %copy-start.19 = (bf16[2,2048,704]{1,2,0:T(8,128)(2,1)S(1)}, bf16[2,2048,704]{1,2,0:T(8,128)(2,1)}, u32[]{:S(2)}) copy-start(bf16[2,2048,704]{1,2,0:T(8,128)(2,1)} %all-gather.9.cloned.1.call-done) | copy-start | bytes 17301508
  288.0 7.3 %copy-start.13 = (bf16[2,88,8,256]{3,2,0,1:T(8,128)(2,1)S(1)}, bf16[2,88,8,256]{3,2,0,1:T(8,128)(2,1)}, u32[]{:S(2)}) copy-start(bf16[2,88,8,256]{3,2,0,1:T(8,128)(2,1)} %copy.79) | copy-start | bytes 2162692
  295.2 2.0 copy-start.8
  297.1 4.2 %collective-permute-start.28 = (bf16[2048,512]{1,0:T(8,128)(2,1)S(1)}, bf16[2048,512]{1,0:T(8,128)(2,1)S(1)}, u32[]{:S(2)}, u32[]{:S(2)}) collective-permute-start(bf16[2048,512]{1,0:T(8,128)(2,1)S(1)} %convolution_convert_fusion), channel_id=1, source_target_pairs={{0,1},{1,0},{2,3},{3,2},{4,5},{5,4},{6,7},{7,6},{8,9},{9,8},{10,11... | collective-permute-start | bytes 6291464 | tf_op jit(solution)/shard_map/ppermute | solution.py:242
  297.3 2.5 copy-start.7
  297.3 2.5 copy-start.6
  299.2 7.1 %collective-permute-start.27 = (bf16[2048,512]{1,0:T(8,128)(2,1)S(1)}, bf16[2048,512]{1,0:T(8,128)(2,1)S(1)}, u32[]{:S(2)}, u32[]{:S(2)}) collective-permute-start(bf16[2048,512]{1,0:T(8,128)(2,1)S(1)} %convolution_convert_fusion.2), channel_id=1, source_target_pairs={{0,1},{1,0},{2,3},{3,2},{4,5},{5,4},{6,7},{7,6},{8,9},{9,8},{10,11... | collective-permute-start | bytes 6291464 | tf_op jit(solution)/shard_map/ppermute | solution.py:242
  303.3 14.0 %collective-permute-start.29 = (bf16[512,512]{1,0:T(8,128)(2,1)S(1)}, bf16[512,512]{1,0:T(8,128)(2,1)S(1)}, u32[]{:S(2)}, u32[]{:S(2)}) collective-permute-start(bf16[512,512]{1,0:T(8,128)(2,1)S(1)} %get-tuple-element.9), channel_id=1, source_target_pairs={{0,4},{4,0},{8,12},{12,8},{16,20},{20,16},{24,28},{28,24},{1,5},{5... | collective-permute-start | bytes 1572872 | tf_op jit(solution)/shard_map/ppermute | solution.py:239
  304.9 14.3 %collective-permute-start.31 = (bf16[512,512]{1,0:T(8,128)(2,1)S(1)}, bf16[512,512]{1,0:T(8,128)(2,1)S(1)}, u32[]{:S(2)}, u32[]{:S(2)}) collective-permute-start(bf16[512,512]{1,0:T(8,128)(2,1)S(1)} %get-tuple-element.10), channel_id=1, source_target_pairs={{0,2},{1,3},{2,0},{3,1},{4,6},{5,7},{6,4},{7,5},{8,10},{9,11},{10,... | collective-permute-start | bytes 1572872 | tf_op jit(solution)/shard_map/ppermute | solution.py:242
  317.6 24.4 %collective-permute-start.30 = (bf16[1024,512]{1,0:T(8,128)(2,1)S(1)}, bf16[1024,512]{1,0:T(8,128)(2,1)S(1)}, u32[]{:S(2)}, u32[]{:S(2)}) collective-permute-start(bf16[1024,512]{1,0:T(8,128)(2,1)S(1)} %pad_maximum_fusion.2), channel_id=1, source_target_pairs={{0,2},{1,3},{2,0},{3,1},{4,6},{5,7},{6,4},{7,5},{8,10},{9,11},{10,... | collective-permute-start | bytes 3145736 | tf_op jit(solution)/shard_map/ppermute | solution.py:242
  319.5 24.1 %collective-permute-start.32 = (bf16[1024,512]{1,0:T(8,128)(2,1)S(1)}, bf16[1024,512]{1,0:T(8,128)(2,1)S(1)}, u32[]{:S(2)}, u32[]{:S(2)}) collective-permute-start(bf16[1024,512]{1,0:T(8,128)(2,1)S(1)} %pad_maximum_fusion.3), channel_id=1, source_target_pairs={{0,4},{4,0},{8,12},{12,8},{16,20},{20,16},{24,28},{28,24},{1,5},{5... | collective-permute-start | bytes 3145736 | tf_op jit(solution)/shard_map/ppermute | solution.py:239
Sparse Core Ops, SparseCore 0:
  16.1 36.2 all-gather.6
  54.0 58.1 all-gather.4
  113.7 57.7 all-gather.10
  172.9 105.3 all-gather.8
